TPU v7x, 512 devices: a 4x2x32 block of a 4x8x32 slice. The times are simulated.
512 devices in a mesh: grp: 2 (over y), fs: 32 (over z), tp: 8 (over x, core).
Axes of the slice: x: 4, y: 2, z: 32, core: 2. Of those that a mesh axis runs over, the one named last changes fastest.
The devices are a block of a 4x8x32 slice.
Arguments:
- tokens: bfloat16 [12288, 2048], P(('grp', 'fs'), 'tp'), parts along dimension 0, may hold values from -40 to 40
- routes: int32 [12288, 8], P(('grp', 'fs')), parts along dimension 0, may hold values from 0 to 31, all different within a row; in each aligned block of 192 rows (0 to 191, 192 to 383, ...) at most 56 rows name the same one
- routing_weight: float32 [12288, 8], P(('grp', 'fs')), parts along dimension 0, may hold values from 0.1 to 0.6
- norm_gain_vector: float32 [2048], P('tp'), may hold values from 0.1 to 1.9
- expert_gate: float32 [32, 512, 2048], P(None, 'fs', 'tp'), may hold values from -0.125 to 0.125
- expert_up: float32 [32, 512, 2048], P(None, 'fs', 'tp'), may hold values from -0.125 to 0.125
- expert_down: float32 [32, 512, 2048], P(None, 'fs', 'tp'), may hold values from -0.25 to 0.25
- shared_gate: float32 [512, 2048], P('fs', 'tp'), may hold values from -0.125 to 0.125
- shared_up: float32 [512, 2048], P('fs', 'tp'), may hold values from -0.125 to 0.125
- shared_down: float32 [512, 2048], P('fs', 'tp'), may hold values from -0.25 to 0.25
Outputs:
- mixed: bfloat16 [12288, 2048], P(('grp', 'fs'), 'tp'), parts along dimension 0
- gate_served: bfloat16 [64, 512, 2048], P(('grp', 'fs'), None, 'tp'), parts along dimension 0
- up_served: bfloat16 [64, 512, 2048], P(('grp', 'fs'), None, 'tp'), parts along dimension 0
- down_served: bfloat16 [64, 512, 2048], P(('grp', 'fs'), None, 'tp'), parts along dimension 0
- shared_gate_served: bfloat16 [1024, 2048], P('grp', 'tp'), parts along dimension 0
- shared_up_served: bfloat16 [1024, 2048], P('grp', 'tp'), parts along dimension 0
- shared_down_served: bfloat16 [1024, 2048], P('grp', 'tp'), parts along dimension 0
There are 2 independent parts, one for each index of `grp`. A program takes and returns all parts, laid end to end along the dimension named above; an argument that names none is the same for every part. Nothing has to cross between parts.
Inputs may be any that keep to these rules, and one draw needn't show every extreme that they name: `routes`: each row names 8 different experts. In each aligned block of 192 rows no expert is named by more than 56 rows, and in some block an expert is named by exactly 56 rows.
All inputs are finite; a program needn't handle non-finite values.
Results may differ from a plain program's by a relative error of at most 0.022.
Values may be sent and summed in bfloat16 or wider, within the bound.
No kernel may reach another device: no remote copies, remote signals or barrier semaphores. Data moves between devices by JAX's collectives and lax.ppermute only.
A program may use at most 64 MiB of HBM per device.

v0:
```python
import jax
import jax.numpy as jnp
from jax import lax
from jax.sharding import PartitionSpec as P

norm_eps = 1e-06


def sent_together(arrays, axis, split_dim, concat_dim, along):
    widths = [a.shape[along] for a in arrays]
    both = jnp.concatenate(arrays, axis=along)
    out = lax.all_to_all(both, axis, split_axis=split_dim, concat_axis=concat_dim, tiled=True)
    return tuple(jnp.split(out, [sum(widths[:k]) for k in range(1, len(widths))], axis=along))


def sent_together_2(arrays, axis, dim, along):
    both = jnp.concatenate(arrays, axis=along)
    out, at, outs = (lax.all_gather(both, axis, axis=dim, tiled=True), 0, [])
    for a in arrays:
        outs.append(lax.slice_in_dim(out, at, at + a.shape[along], axis=along))
        at += a.shape[along]
    return tuple(outs)


def in_one_piece(arrays, axis, dim, along):
    both = jnp.concatenate(arrays, axis=along)
    out, at, outs = (lax.psum_scatter(both, axis, scatter_dimension=dim, tiled=True), 0, [])
    for a in arrays:
        outs.append(lax.slice_in_dim(out, at, at + a.shape[along], axis=along))
        at += a.shape[along]
    return tuple(outs)


def dense_rows(rows, weight):
    return lax.dot_general(
        rows, weight, (((1,), (1,)), ((), ())), preferred_element_type=jnp.float32
    )


def per_device(
    tokens,
    routes,
    routing_weight,
    norm_gain_vector,
    expert_gate,
    expert_up,
    expert_down,
    shared_gate,
    shared_up,
    shared_down,
):
    tok_rows, portion_width = tokens.shape
    model_width = portion_width * lax.axis_size("tp")
    experts = expert_gate.shape[0]
    top_count = routes.shape[1]
    capacity = tok_rows * top_count * 7 // (6 * experts)
    gate_round = (expert_gate * norm_gain_vector[None, None, :]).astype(jnp.bfloat16)
    up_round = (expert_up * norm_gain_vector[None, None, :]).astype(jnp.bfloat16)
    down_round = expert_down.astype(jnp.bfloat16)
    gate_refreshed, up_new, down_new = sent_together(
        (gate_round, up_round, down_round), "fs", 0, 1, 2
    )
    shared_g, shared_u, shared_d = sent_together_2(
        (
            (shared_gate * norm_gain_vector[None, :]).astype(jnp.bfloat16),
            (shared_up * norm_gain_vector[None, :]).astype(jnp.bfloat16),
            shared_down.astype(jnp.bfloat16),
        ),
        "fs",
        0,
        1,
    )
    values = tokens.astype(jnp.float32)
    totals = lax.psum(jnp.sum(values * values, axis=1), "tp")
    normed = (values * lax.rsqrt(totals / model_width + norm_eps)[:, None]).astype(jnp.bfloat16)
    flat_expert = routes.reshape(-1)
    onehot = (flat_expert[:, None] == jnp.arange(experts, dtype=jnp.int32)[None, :]).astype(
        jnp.int32
    )
    earlier = jnp.cumsum(onehot, axis=0) - onehot
    slot_index = jnp.sum(earlier * onehot, axis=1)
    target = (flat_expert * capacity + slot_index).reshape(tok_rows, top_count)
    places = jnp.arange(experts * capacity, dtype=jnp.int32)
    placing = jnp.sum(
        (target[:, :, None] == places[None, None, :]).astype(jnp.int32), axis=1
    ).astype(jnp.bfloat16)
    outgoing = lax.dot_general(
        placing, normed, (((0,), (0,)), ((), ())), preferred_element_type=jnp.float32
    ).astype(jnp.bfloat16)
    incoming = lax.all_to_all(
        outgoing.reshape(experts, capacity, portion_width),
        "fs",
        split_axis=0,
        concat_axis=0,
        tiled=True,
    )
    arrived = incoming.reshape(experts * capacity, portion_width)
    partials = (
        dense_rows(arrived, gate_refreshed[0]).astype(jnp.bfloat16),
        dense_rows(arrived, up_new[0]).astype(jnp.bfloat16),
        dense_rows(normed, shared_g).astype(jnp.bfloat16),
        dense_rows(normed, shared_u).astype(jnp.bfloat16),
    )
    gate_part, up_part, sgate_part, sup_part = tuple(
        (
            part.astype(jnp.float32)
            for part in in_one_piece(
                (partials[0], partials[1], partials[2], partials[3]), "tp", 1, 0
            )
        )
    )
    hidden, shared_hidden = (
        lax.all_gather(
            (jax.nn.silu(gate_part) * up_part).astype(jnp.bfloat16), "tp", axis=1, tiled=True
        ),
        lax.all_gather(
            (jax.nn.silu(sgate_part) * sup_part).astype(jnp.bfloat16), "tp", axis=1, tiled=True
        ),
    )
    produced = jnp.dot(hidden, down_new[0], preferred_element_type=jnp.float32).astype(jnp.bfloat16)
    returned = lax.all_to_all(
        produced.reshape(experts, capacity, portion_width),
        "fs",
        split_axis=0,
        concat_axis=0,
        tiled=True,
    )
    picked = returned.reshape(experts * capacity, portion_width)[target]
    routed = jnp.sum(routing_weight[:, :, None] * picked.astype(jnp.float32), axis=1)
    shared_out = jnp.dot(shared_hidden, shared_d, preferred_element_type=jnp.float32)
    mixed = (routed + shared_out).astype(jnp.bfloat16)
    return (mixed, gate_refreshed, up_new, down_new, shared_g, shared_u, shared_d)


def solution(mesh):
    return jax.shard_map(
        per_device,
        mesh=mesh,
        in_specs=(
            P(("grp", "fs"), "tp"),
            P(("grp", "fs"), None),
            P(("grp", "fs"), None),
            P("tp"),
            P(None, "fs", "tp"),
            P(None, "fs", "tp"),
            P(None, "fs", "tp"),
            P("fs", "tp"),
            P("fs", "tp"),
            P("fs", "tp"),
        ),
        out_specs=(
            P(("grp", "fs"), "tp"),
            P(("grp", "fs"), None, "tp"),
            P(("grp", "fs"), None, "tp"),
            P(("grp", "fs"), None, "tp"),
            P("grp", "tp"),
            P("grp", "tp"),
            P("grp", "tp"),
        ),
        check_vma=False,
    )
```

profile of v0, /device:TPU:33, one launch (start us, length us, event | category | flops | bytes accessed | tf_op | source)
XLA Modules:
  0.0 525.0 jit_solution(1667189688354686824)
XLA Ops:
  7.2 1.1 convert_element_type.88
  8.3 1.3 multiply_convert_fusion.1
  9.6 1.0 pad_maximum_fusion.1
  10.6 46.3 %all-to-all-start.1 = ((bf16[32,16,768]{2,1,0:T(8,128)(2,1)}), bf16[32,16,768]{2,1,0:T(8,128)(2,1)S(1)}, u32[]{:S(2)}, u32[]{:S(2)}) async-start(bf16[32,16,768]{2,1,0:T(8,128)(2,1)} %pad_maximum_fusion.1), calls=%async_computation.1 | async-start | bytes 1572864 | tf_op jit(solution)/shard_map/all_to_all | solution.py:12
  56.9 0.1 copy.45
  57.0 0.1 eq.42
  57.1 0.1 eq.38
  57.3 9.1 %reduce-window.6 = s32[32,12,128]{2,1,0:T(8,128)S(1)} reduce-window(s32[32,12,128]{2,1,0:T(8,128)S(1)} %fusion.11, s32[]{:T(128)} %constant.6.clone.1), window={size=1x1x128 pad=0_0x0_0x127_0}, to_apply=%region_0.0 | reduce-window | flops 6242304 | bytes 393220 | tf_op jit(solution)/shard_map/reduce-window
  66.4 0.1 slice.38
  66.5 0.2 copy.47
  66.7 0.1 copy.48
  66.8 0.1 broadcast_add_fusion
  66.9 0.1 fusion.16
  67.0 0.1 reduce_sum.39
  67.1 0.1 copy.49
  67.2 0.1 copy.50
  67.3 0.1 fusion.12
  67.5 13.3 %psum.7 = f32[192]{0:T(256)S(1)} all-reduce(f32[192]{0:T(256)S(1)} %fusion.12), channel_id=1, replica_groups=mesh['grp'=2,'fs'=32,'tp'=8] {'tp'}, use_global_device_ids=true, to_apply=%region_5.6 | all-reduce | flops 192 | bytes 1536 | tf_op jit(solution)/shard_map/psum | solution.py:74
  80.8 5.0 convert_reduce_fusion
  85.9 1.5 convolution_convert_fusion.3
  87.3 55.5 %all-to-all-done.1 = bf16[32,16,768]{2,1,0:T(8,128)(2,1)S(1)} async-done(((bf16[32,16,768]{2,1,0:T(8,128)(2,1)}), bf16[32,16,768]{2,1,0:T(8,128)(2,1)S(1)}, u32[]{:S(2)}, u32[]{:S(2)}) %all-to-all-start.1) | async-done | bytes 786464 | tf_op jit(solution)/shard_map/all_to_all | solution.py:12
  142.8 4.8 all-to-all-start
  147.7 0.1 reduce-scatter.4.cloned.1.call-start
  147.8 122.6 %all_gather.9 = bf16[512,768]{1,0:T(8,128)(2,1)S(1)} all-gather(bf16[16,768]{1,0:T(8,128)(2,1)S(1)} %pad_maximum_fusion.2), channel_id=1, replica_groups=mesh['grp'=2,'fs'=32,'tp'=8] {'fs'}, dimensions={0}, use_global_device_ids=true | all-gather | bytes 811008 | tf_op jit(solution)/shard_map/all_gather | solution.py:18
  270.5 0.2 convolution_convert_fusion.4
  270.7 0.9 convolution_convert_fusion.5
  271.8 0.7 convolution_convert_fusion
  272.5 0.7 convolution_convert_fusion.1
  273.2 0.2 copy-done.6
  273.4 2.1 pad_maximum_fusion
  275.5 6.3 %copy.56 = bf16[3968,512]{0,1:T(8,128)(2,1)} copy(bf16[3968,512]{1,0:T(8,128)(2,1)} %pad_maximum_fusion) | data formatting | bytes 8126464
  281.8 0.1 reduce-scatter.4.cloned.1.call-update
  281.8 0.2 all-gather.2.cloned.1.call-start
  282.1 64.3 %reduce-scatter.4.cloned.1.call-done = bf16[64,3968]{1,0:T(8,128)(2,1)} async-done(((bf16[512,3968]{1,0:T(8,128)(2,1)}), bf16[64,3968]{1,0:T(8,128)(2,1)}) %reduce-scatter.4.cloned.1.call-update) | async-done | bytes 507920
  346.4 1.9 fusion.7
  348.3 0.1 all-gather.2.cloned.1.call-update
  348.3 41.7 %all-gather.2.cloned.1.call-done = bf16[1792,512]{0,1:T(8,128)(2,1)} async-done(((bf16[1792,64]{0,1:T(8,128)(2,1)}), bf16[1792,512]{0,1:T(8,128)(2,1)}) %all-gather.2.cloned.1.call-update) | async-done | bytes 1835024 | tf_op jit(solution)/shard_map/all_gather | solution.py:113
  390.0 3.1 convolution_convert_fusion.2
  393.1 23.3 %all-to-all-start.2 = ((bf16[32,56,256]{2,1,0:T(8,128)(2,1)}), bf16[32,56,256]{2,1,0:T(8,128)(2,1)S(1)}, u32[]{:S(2)}, u32[]{:S(2)}) async-start(bf16[32,56,256]{2,1,0:T(8,128)(2,1)} %bitcast.8), calls=%async_computation.2 | async-start | bytes 1835008 | tf_op jit(solution)/shard_map/all_to_all | solution.py:121
  416.5 0.1 copy.53
  416.6 0.1 reshape.66
  416.7 0.1 copy.44
  416.8 0.9 fusion.21
  417.7 13.4 %all_gather.11 = bf16[192,512]{0,1:T(8,128)(2,1)S(1)} all-gather(bf16[192,64]{0,1:T(8,128)(2,1)S(1)} %fusion.21), channel_id=1, replica_groups=mesh['grp'=2,'fs'=32,'tp'=8] {'tp'}, dimensions={1}, use_global_device_ids=true | all-gather | bytes 221184 | tf_op jit(solution)/shard_map/all_gather | solution.py:116
  431.2 80.7 %all-to-all-done.2 = bf16[32,56,256]{2,1,0:T(8,128)(2,1)S(1)} async-done(((bf16[32,56,256]{2,1,0:T(8,128)(2,1)}), bf16[32,56,256]{2,1,0:T(8,128)(2,1)S(1)}, u32[]{:S(2)}, u32[]{:S(2)}) %all-to-all-start.2) | async-done | bytes 917536 | tf_op jit(solution)/shard_map/all_to_all | solution.py:121
  511.9 4.8 gather_fusion
  516.7 0.5 fusion
  517.2 0.9 fusion.1
  (38 shorter events, 0.3 us)
Async XLA Ops:
  9.6 47.3 %copy-start.8 = (s32[192,8]{0,1:T(8,128)S(1)}, s32[192,8]{0,1:T(8,128)}, u32[]{:S(2)}) copy-start(s32[192,8]{0,1:T(8,128)} %param.11) | copy-start | bytes 18436
  10.6 132.3 %all-to-all-start.1 = ((bf16[32,16,768]{2,1,0:T(8,128)(2,1)}), bf16[32,16,768]{2,1,0:T(8,128)(2,1)S(1)}, u32[]{:S(2)}, u32[]{:S(2)}) async-start(bf16[32,16,768]{2,1,0:T(8,128)(2,1)} %pad_maximum_fusion.1), calls=%async_computation.1 | async-start | bytes 1572864 | tf_op jit(solution)/shard_map/all_to_all | solution.py:12
  56.9 10.4 %copy-start = (bf16[192,256]{1,0:T(8,128)(2,1)S(1)}, bf16[192,256]{1,0:T(8,128)(2,1)}, u32[]{:S(2)}) copy-start(bf16[192,256]{1,0:T(8,128)(2,1)} %param.10) | copy-start | bytes 294916
  85.8 61.9 %copy-start.11 = (f32[16,256]{1,0:T(8,128)S(1)}, f32[16,256]{1,0:T(8,128)}, u32[]{:S(2)}) copy-start(f32[16,256]{1,0:T(8,128)} %param.19) | copy-start | bytes 49156
  85.8 62.0 %copy-start.9 = (f32[16,256]{1,0:T(8,128)S(1)}, f32[16,256]{1,0:T(8,128)}, u32[]{:S(2)}) copy-start(f32[16,256]{1,0:T(8,128)} %param.17) | copy-start | bytes 49156
  85.8 62.0 %copy-start.10 = (f32[16,256]{1,0:T(8,128)S(1)}, f32[16,256]{1,0:T(8,128)}, u32[]{:S(2)}) copy-start(f32[16,256]{1,0:T(8,128)} %param.18) | copy-start | bytes 49156
  85.9 62.0 %copy-start.13 = (f32[256]{0:T(256)S(1)}, f32[256]{0:T(256)}, u32[]{:S(2)}) copy-start(f32[256]{0:T(256)} %param.13) | copy-start | bytes 3076
  142.8 128.9 %all-to-all-start = ((bf16[32,56,256]{2,1,0:T(8,128)(2,1)}), bf16[32,56,256]{2,1,0:T(8,128)(2,1)S(1)}, u32[]{:S(2)}, u32[]{:S(2)}) async-start(bf16[32,56,256]{2,1,0:T(8,128)(2,1)} %bitcast.2), calls=%async_computation | async-start | bytes 1835008 | tf_op jit(solution)/shard_map/all_to_all | solution.py:90
  147.7 198.7 %reduce-scatter.4.cloned.1.call-start = ((), (), s32[]{:S(2)}) async-start(), calls=%async_computation.5 | async-start | bytes 4571136
  270.5 2.0 copy-start.4
  270.5 2.0 copy-start.5
  270.5 246.7 %copy-start.1 = (bf16[512,256]{1,0:T(8,128)(2,1)}, bf16[512,256]{1,0:T(8,128)(2,1)S(1)}, u32[]{:S(2)}) copy-start(bf16[512,256]{1,0:T(8,128)(2,1)S(1)} %get-tuple-element.9) | copy-start | bytes 786436
  271.7 1.4 copy-start.2
  271.7 1.4 copy-start.3
  271.8 118.2 %copy-start.7 = (bf16[1,512,256]{2,1,0:T(8,128)(2,1)}, bf16[1,512,256]{2,1,0:T(8,128)(2,1)S(1)}, u32[]{:S(2)}) copy-start(bf16[1,512,256]{2,1,0:T(8,128)(2,1)S(1)} %get-tuple-element.12) | copy-start | bytes 786436
  272.5 0.9 copy-start.6
  281.8 108.2 %all-gather.2.cloned.1.call-start = ((), (), s32[]{:S(2)}) async-start(), calls=%async_computation.4 | async-start | bytes 2064384 | tf_op jit(solution)/shard_map/all_gather | solution.py:113
  393.1 23.6 %copy-start.12 = (f32[192,8]{0,1:T(8,128)S(1)}, f32[192,8]{0,1:T(8,128)}, u32[]{:S(2)}) copy-start(f32[192,8]{0,1:T(8,128)} %param.12) | copy-start | bytes 18436
  393.1 118.8 %all-to-all-start.2 = ((bf16[32,56,256]{2,1,0:T(8,128)(2,1)}), bf16[32,56,256]{2,1,0:T(8,128)(2,1)S(1)}, u32[]{:S(2)}, u32[]{:S(2)}) async-start(bf16[32,56,256]{2,1,0:T(8,128)(2,1)} %bitcast.8), calls=%async_computation.2 | async-start | bytes 1835008 | tf_op jit(solution)/shard_map/all_to_all | solution.py:121
Sparse Core Ops, SparseCore 0:
  281.9 64.3 reduce-scatter.3
  348.5 41.4 all-gather.1
where the time goes:
time: 526 us; the launch traced here: 525 us
  waiting for transfers between devices  242 us (46%)
  blocking collectives  149 us (28%)
  starting transfers between devices  74.8 us (14%)
  other arithmetic  23.3 us (4%)
  between operations  14.5 us (3%)
  local copies, waits for them, and re-layouts  12.8 us (2%)
  matrix products  8.01 us (2%)
    all_gather x1, blocking collectives, sent_together_2(): out, at, outs = (lax.all_gather(both, axis, axis=dim, tiled=True), 0, [])  123 us
    all_to_all x1, waiting for transfers between devices, per_device(): lax.all_to_all(produced.reshape(experts, capacity, portion_width), 'fs',...  80.7 us
    unnamed x3, waiting for transfers between devices  64.4 us
    all_to_all x1, waiting for transfers between devices, sent_together(): lax.all_to_all(both, axis, split_axis=split_dim, concat_axis=concat_dim,...  55.5 us
    all_to_all x1, starting transfers between devices, sent_together(): lax.all_to_all(both, axis, split_axis=split_dim, concat_axis=concat_dim,...  46.3 us
    all_gather x1, waiting for transfers between devices, per_device(): lax.all_gather((jax.nn.silu(gate_part) * up_part).astype(jnp.bfloat16), '...  41.7 us
    all_to_all x1, starting transfers between devices, per_device(): lax.all_to_all(produced.reshape(experts, capacity, portion_width), 'fs',...  23.3 us
    all_gather x1, blocking collectives, per_device(): lax.all_gather((jax.nn.silu(sgate_part) * sup_part).astype(jnp.bfloat16),...  13.4 us
  transfers between devices with their start and end apart: 5, of which 4 were waited for; matrix products, arithmetic and copies ran while one was open for 4% of the time, Pallas kernels for 0%

commit v1 on v0

--- a/solution.py
+++ b/solution.py
@@ -110,8 +110,16 @@
         )
     )
     hidden, shared_hidden = (
-        lax.all_gather(
-            (jax.nn.silu(gate_part) * up_part).astype(jnp.bfloat16), "tp", axis=1, tiled=True
+        jnp.concatenate(
+            lax.all_to_all(
+                jnp.stack(
+                    [(jax.nn.silu(gate_part) * up_part).astype(jnp.bfloat16)] * lax.axis_size("tp")
+                ),
+                "tp",
+                0,
+                0,
+            ),
+            axis=1,
         ),
         lax.all_gather(
             (jax.nn.silu(sgate_part) * sup_part).astype(jnp.bfloat16), "tp", axis=1, tiled=True

time: 526 us -> 509 us (0.968)
  waiting for transfers between devices: 242 us -> 200 us
  blocking collectives: 149 us -> 179 us
    all_gather x1 -> x0, waiting for transfers between devices: 41.7 us -> none  [per_device(): lax.all_gather((jax.nn.silu(gate_part) * up_part).astype(jnp.bfloat16), '...]
    all_to_all x0 -> x1, blocking collectives: none -> 28.6 us  [per_device(): lax.all_to_all(jnp.stack([(jax.nn.silu(gate_part) * up_part).astype(jnp.b...]
    unnamed x3 -> x2, waiting for transfers between devices: 64.4 us -> 64.6 us
  transfers between devices with their start and end apart: 5 -> 4, of which waited for: 4 -> 3; matrix products, arithmetic and copies ran while one was open for 4% -> 4% of each run, Pallas kernels for 0% -> 0%
where the time goes in v1:
time: 509 us; the launch traced here: 508 us
  waiting for transfers between devices  200 us (39%)
  blocking collectives  179 us (35%)
  starting transfers between devices  73.3 us (14%)
  other arithmetic  22.6 us (4%)
  between operations  14.5 us (3%)
  local copies, waits for them, and re-layouts  12.9 us (3%)
  matrix products  6.46 us (1%)
    all_gather x1, blocking collectives, sent_together_2(): out, at, outs = (lax.all_gather(both, axis, axis=dim, tiled=True), 0, [])  123 us
    all_to_all x1, waiting for transfers between devices, per_device(): lax.all_to_all(produced.reshape(experts, capacity, portion_width), 'fs',...  79.5 us
    unnamed x2, waiting for transfers between devices  64.6 us
    all_to_all x1, waiting for transfers between devices, sent_together(): lax.all_to_all(both, axis, split_axis=split_dim, concat_axis=concat_dim,...  55.5 us
    all_to_all x1, starting transfers between devices, sent_together(): lax.all_to_all(both, axis, split_axis=split_dim, concat_axis=concat_dim,...  46.3 us
    all_to_all x1, blocking collectives, per_device(): lax.all_to_all(jnp.stack([(jax.nn.silu(gate_part) * up_part).astype(jnp.b...  28.6 us
    all_to_all x1, starting transfers between devices, per_device(): lax.all_to_all(produced.reshape(experts, capacity, portion_width), 'fs',...  22.1 us
    all_gather x1, blocking collectives, per_device(): lax.all_gather((jax.nn.silu(sgate_part) * sup_part).astype(jnp.bfloat16),...  14.2 us
  transfers between devices with their start and end apart: 4, of which 3 were waited for; matrix products, arithmetic and copies ran while one was open for 4% of the time, Pallas kernels for 0%

profile of v1, /device:TPU:33, one launch (start us, length us, event | category | flops | bytes accessed | tf_op | source)
XLA Modules:
  0.0 508.0 jit_solution(9677543404593068625)
XLA Ops:
  7.2 1.1 convert_element_type.88
  8.3 1.3 multiply_convert_fusion.1
  9.6 1.0 pad_maximum_fusion.1
  10.6 46.3 %all-to-all-start.1 = ((bf16[32,16,768]{2,1,0:T(8,128)(2,1)}), bf16[32,16,768]{2,1,0:T(8,128)(2,1)S(1)}, u32[]{:S(2)}, u32[]{:S(2)}) async-start(bf16[32,16,768]{2,1,0:T(8,128)(2,1)} %pad_maximum_fusion.1), calls=%async_computation.1 | async-start | bytes 1572864 | tf_op jit(solution)/shard_map/all_to_all | solution.py:12
  56.9 0.1 copy.46
  57.0 0.1 eq.42
  57.1 0.1 eq.38
  57.3 9.1 %reduce-window.6 = s32[32,12,128]{2,1,0:T(8,128)S(1)} reduce-window(s32[32,12,128]{2,1,0:T(8,128)S(1)} %fusion.11, s32[]{:T(128)} %constant.6.clone.1), window={size=1x1x128 pad=0_0x0_0x127_0}, to_apply=%region_0.0 | reduce-window | flops 6242304 | bytes 393220 | tf_op jit(solution)/shard_map/reduce-window
  66.3 0.1 slice.38
  66.5 0.2 copy.48
  66.7 0.1 copy.49
  66.8 0.1 broadcast_add_fusion
  66.9 0.1 fusion.16
  67.0 0.1 reduce_sum.39
  67.1 0.1 copy.50
  67.2 0.1 copy.51
  67.3 0.1 fusion.12
  67.4 13.3 %psum.7 = f32[192]{0:T(256)S(1)} all-reduce(f32[192]{0:T(256)S(1)} %fusion.12), channel_id=1, replica_groups=mesh['grp'=2,'fs'=32,'tp'=8] {'tp'}, use_global_device_ids=true, to_apply=%region_5.6 | all-reduce | flops 192 | bytes 1536 | tf_op jit(solution)/shard_map/psum | solution.py:74
  80.8 5.1 convert_reduce_fusion
  85.9 1.4 convolution_convert_fusion.3
  87.3 55.5 %all-to-all-done.1 = bf16[32,16,768]{2,1,0:T(8,128)(2,1)S(1)} async-done(((bf16[32,16,768]{2,1,0:T(8,128)(2,1)}), bf16[32,16,768]{2,1,0:T(8,128)(2,1)S(1)}, u32[]{:S(2)}, u32[]{:S(2)}) %all-to-all-start.1) | async-done | bytes 786464 | tf_op jit(solution)/shard_map/all_to_all | solution.py:12
  142.8 4.8 all-to-all-start
  147.7 0.1 reduce-scatter.4.cloned.1.call-start
  147.8 122.6 %all_gather.6 = bf16[512,768]{1,0:T(8,128)(2,1)S(1)} all-gather(bf16[16,768]{1,0:T(8,128)(2,1)S(1)} %pad_maximum_fusion.2), channel_id=1, replica_groups=mesh['grp'=2,'fs'=32,'tp'=8] {'fs'}, dimensions={0}, use_global_device_ids=true | all-gather | bytes 811008 | tf_op jit(solution)/shard_map/all_gather | solution.py:18
  270.4 0.1 fusion.25
  270.5 0.2 convolution_convert_fusion.4
  270.7 0.9 convolution_convert_fusion.5
  271.8 0.7 convolution_convert_fusion
  272.5 0.7 convolution_convert_fusion.1
  273.2 0.2 copy-done.6
  273.4 2.1 pad_maximum_fusion
  275.4 6.3 %copy.57 = bf16[3968,512]{0,1:T(8,128)(2,1)} copy(bf16[3968,512]{1,0:T(8,128)(2,1)} %pad_maximum_fusion) | data formatting | bytes 8126464
  281.7 0.1 reduce-scatter.4.cloned.1.call-update
  281.8 64.6 %reduce-scatter.4.cloned.1.call-done = bf16[64,3968]{1,0:T(8,128)(2,1)} async-done(((bf16[512,3968]{1,0:T(8,128)(2,1)}), bf16[64,3968]{1,0:T(8,128)(2,1)}) %reduce-scatter.4.cloned.1.call-update) | async-done | bytes 507920
  346.3 1.2 fusion.7
  347.5 0.1 stack.2
  347.7 28.6 %all_to_all.27 = bf16[8,1792,64]{1,2,0:T(8,128)(2,1)S(1)} all-to-all(bf16[8,1792,64]{1,2,0:T(8,128)(2,1)S(1)} %stack.2), channel_id=1, replica_groups=mesh['grp'=2,'fs'=32,'tp'=8] {'tp'}, dimensions={0} | all-to-all | bytes 3670016 | tf_op jit(solution)/shard_map/all_to_all | solution.py:114
  376.3 1.6 convolution_convert_fusion.2
  377.9 22.1 %all-to-all-start.3 = ((bf16[32,56,256]{2,1,0:T(8,128)(2,1)}), bf16[32,56,256]{2,1,0:T(8,128)(2,1)S(1)}, u32[]{:S(2)}, u32[]{:S(2)}) async-start(bf16[32,56,256]{2,1,0:T(8,128)(2,1)} %bitcast.10), calls=%async_computation.3 | async-start | bytes 1835008 | tf_op jit(solution)/shard_map/all_to_all | solution.py:129
  400.0 0.1 copy.54
  400.1 0.1 reshape.76
  400.3 0.1 copy.45
  400.4 0.9 fusion.21
  401.3 14.2 %all_gather.7 = bf16[192,512]{0,1:T(8,128)(2,1)S(1)} all-gather(bf16[192,64]{0,1:T(8,128)(2,1)S(1)} %fusion.21), channel_id=1, replica_groups=mesh['grp'=2,'fs'=32,'tp'=8] {'tp'}, dimensions={1}, use_global_device_ids=true | all-gather | bytes 221184 | tf_op jit(solution)/shard_map/all_gather | solution.py:124
  415.5 79.5 %all-to-all-done.3 = bf16[32,56,256]{2,1,0:T(8,128)(2,1)S(1)} async-done(((bf16[32,56,256]{2,1,0:T(8,128)(2,1)}), bf16[32,56,256]{2,1,0:T(8,128)(2,1)S(1)}, u32[]{:S(2)}, u32[]{:S(2)}) %all-to-all-start.3) | async-done | bytes 917536 | tf_op jit(solution)/shard_map/all_to_all | solution.py:129
  495.0 4.8 gather_fusion
  499.7 0.5 fusion
  500.3 0.9 fusion.1
  (37 shorter events, 0.2 us)
Async XLA Ops:
  9.6 47.3 %copy-start.8 = (s32[192,8]{0,1:T(8,128)S(1)}, s32[192,8]{0,1:T(8,128)}, u32[]{:S(2)}) copy-start(s32[192,8]{0,1:T(8,128)} %param.11) | copy-start | bytes 18436
  10.6 132.3 %all-to-all-start.1 = ((bf16[32,16,768]{2,1,0:T(8,128)(2,1)}), bf16[32,16,768]{2,1,0:T(8,128)(2,1)S(1)}, u32[]{:S(2)}, u32[]{:S(2)}) async-start(bf16[32,16,768]{2,1,0:T(8,128)(2,1)} %pad_maximum_fusion.1), calls=%async_computation.1 | async-start | bytes 1572864 | tf_op jit(solution)/shard_map/all_to_all | solution.py:12
  56.9 10.4 %copy-start = (bf16[192,256]{1,0:T(8,128)(2,1)S(1)}, bf16[192,256]{1,0:T(8,128)(2,1)}, u32[]{:S(2)}) copy-start(bf16[192,256]{1,0:T(8,128)(2,1)} %param.10) | copy-start | bytes 294916
  85.8 61.9 %copy-start.11 = (f32[16,256]{1,0:T(8,128)S(1)}, f32[16,256]{1,0:T(8,128)}, u32[]{:S(2)}) copy-start(f32[16,256]{1,0:T(8,128)} %param.19) | copy-start | bytes 49156
  85.9 61.9 %copy-start.9 = (f32[16,256]{1,0:T(8,128)S(1)}, f32[16,256]{1,0:T(8,128)}, u32[]{:S(2)}) copy-start(f32[16,256]{1,0:T(8,128)} %param.17) | copy-start | bytes 49156
  85.9 61.9 %copy-start.10 = (f32[16,256]{1,0:T(8,128)S(1)}, f32[16,256]{1,0:T(8,128)}, u32[]{:S(2)}) copy-start(f32[16,256]{1,0:T(8,128)} %param.18) | copy-start | bytes 49156
  85.9 61.9 %copy-start.13 = (f32[256]{0:T(256)S(1)}, f32[256]{0:T(256)}, u32[]{:S(2)}) copy-start(f32[256]{0:T(256)} %param.13) | copy-start | bytes 3076
  142.8 128.9 %all-to-all-start = ((bf16[32,56,256]{2,1,0:T(8,128)(2,1)}), bf16[32,56,256]{2,1,0:T(8,128)(2,1)S(1)}, u32[]{:S(2)}, u32[]{:S(2)}) async-start(bf16[32,56,256]{2,1,0:T(8,128)(2,1)} %bitcast.2), calls=%async_computation | async-start | bytes 1835008 | tf_op jit(solution)/shard_map/all_to_all | solution.py:90
  147.7 198.7 %reduce-scatter.4.cloned.1.call-start = ((), (), s32[]{:S(2)}) async-start(), calls=%async_computation.5 | async-start | bytes 4571136
  270.4 2.0 copy-start.4
  270.4 2.0 copy-start.5
  270.5 229.8 %copy-start.1 = (bf16[512,256]{1,0:T(8,128)(2,1)}, bf16[512,256]{1,0:T(8,128)(2,1)S(1)}, u32[]{:S(2)}) copy-start(bf16[512,256]{1,0:T(8,128)(2,1)S(1)} %get-tuple-element.9) | copy-start | bytes 786436
  271.7 1.4 copy-start.2
  271.7 1.4 copy-start.3
  271.7 104.5 %copy-start.7 = (bf16[1,512,256]{2,1,0:T(8,128)(2,1)}, bf16[1,512,256]{2,1,0:T(8,128)(2,1)S(1)}, u32[]{:S(2)}) copy-start(bf16[1,512,256]{2,1,0:T(8,128)(2,1)S(1)} %get-tuple-element.12) | copy-start | bytes 786436
  272.5 0.9 copy-start.6
  377.9 22.4 %copy-start.12 = (f32[192,8]{0,1:T(8,128)S(1)}, f32[192,8]{0,1:T(8,128)}, u32[]{:S(2)}) copy-start(f32[192,8]{0,1:T(8,128)} %param.12) | copy-start | bytes 18436
  377.9 117.1 %all-to-all-start.3 = ((bf16[32,56,256]{2,1,0:T(8,128)(2,1)}), bf16[32,56,256]{2,1,0:T(8,128)(2,1)S(1)}, u32[]{:S(2)}, u32[]{:S(2)}) async-start(bf16[32,56,256]{2,1,0:T(8,128)(2,1)} %bitcast.10), calls=%async_computation.3 | async-start | bytes 1835008 | tf_op jit(solution)/shard_map/all_to_all | solution.py:129
Sparse Core Ops, SparseCore 0:
  281.9 64.3 reduce-scatter.3
